TPU v7x, 32 devices: a whole 2x2x4 slice. The times are simulated.
32 devices in a mesh: ep: 8 (over z, y), tp: 4 (over x, core).
Axes of the slice: x: 2, y: 2, z: 4, core: 2. Of those that a mesh axis runs over, the one named last changes fastest.
Arguments:
- queries: bfloat16 [2048, 768], P('ep', 'tp'), may hold values from -270 to 270
- key_rows: bfloat16 [2048, 256], P('ep', 'tp'), may hold values from -6 to 6
- value_rows: bfloat16 [2048, 256], P('ep', 'tp'), may hold values from -6 to 6
- sink_logits: float32 [12], P('tp'), may hold values from 2 to 6
- out_weight: bfloat16 [768, 2048], P('tp'), may hold values from -0.21875 to 0.21875
- mix_gain: float32 [2048], replicated, may hold values from 0.1 to 1.9
- moe_tokens: bfloat16 [4096, 2048], P(('ep', 'tp')), may hold values from -600 to 600
- moe_gain: float32 [2048], replicated, may hold values from 0.1 to 1.9
- routes: int32 [4096, 2], P(('ep', 'tp')), may hold values from 0 to 7, all different within a row; in each aligned block of 128 rows (0 to 127, 128 to 255, ...) at most 40 rows name the same one
- route_weights: float32 [4096, 2], P(('ep', 'tp')), may hold values from 0.25 to 1.5
- expert_gate: bfloat16 [8, 2048, 3584], P('ep', None, 'tp'), may hold values from -0.125 to 0.125
- expert_up: bfloat16 [8, 2048, 3584], P('ep', None, 'tp'), may hold values from -0.125 to 0.125
- expert_down: bfloat16 [8, 3584, 2048], P('ep', 'tp'), may hold values from -0.09375 to 0.09375
Outputs:
- mixed: bfloat16 [2048, 2048], P(('ep', 'tp'))
- moe_out: bfloat16 [4096, 2048], P(('ep', 'tp'))
Inputs may be any that keep to these rules, and one draw needn't show every extreme that they name: `routes`: each row names 2 different experts. In the rows of one device no expert is named more than 40 times, and in every draw some device names some expert exactly 40 times.
All inputs are finite; a program needn't handle non-finite values.
Results may differ from a plain program's by a relative error of at most 0.012.
Values may be sent and summed in bfloat16 or wider, within the bound.
No kernel may reach another device: no remote copies, remote signals or barrier semaphores. Data moves between devices by JAX's collectives and lax.ppermute only.
A program may use at most 128 MiB of HBM per device.

v0:
```python
import jax
import jax.numpy as jnp
from jax import lax
from jax.sharding import PartitionSpec as P

HDIM = 64
WINDOW = 128


norm_eps = 1e-06
masked_value = -1e30


def shifted(shard, axis, by):
    size = lax.axis_size(axis)
    pairs = [(i, i + by) for i in range(size) if 0 <= i + by < size]
    return lax.ppermute(shard, axis, pairs)


def rms_scale(rows_in, gain):
    squares = jnp.mean(rows_in * rows_in, axis=-1, keepdims=True)
    return rows_in * lax.rsqrt(squares + norm_eps) * gain


def mixer(queries, key_rows, value_rows, sink_logits, out_weight, mix_gain):
    tok_rows = queries.shape[0]
    kv_local = key_rows.shape[1] // HDIM
    group_size = queries.shape[1] // key_rows.shape[1]
    rim_rows = (key_rows[tok_rows - WINDOW :], value_rows[tok_rows - WINDOW :])
    prev_keys, prev_values = shifted((rim_rows[0], rim_rows[1]), "ep", 1)
    all_keys = jnp.concatenate([prev_keys, key_rows], axis=0).reshape(
        tok_rows + WINDOW, kv_local, HDIM
    )
    all_values = jnp.concatenate([prev_values, value_rows], axis=0).reshape(
        tok_rows + WINDOW, kv_local, HDIM
    )
    offset = lax.axis_index("ep") * tok_rows
    query_pos = offset + jnp.arange(tok_rows, dtype=jnp.int32)
    key_pos = offset - WINDOW + jnp.arange(tok_rows + WINDOW, dtype=jnp.int32)
    distance = query_pos[:, None] - key_pos[None, :]
    allowed = (distance >= 0) & (distance < WINDOW) & (key_pos >= 0)[None, :]
    grouped = queries.reshape(tok_rows, kv_local, group_size, HDIM)
    scores = jnp.einsum(
        "qkgd,jkd->kgqj", grouped, all_keys, preferred_element_type=jnp.float32
    ) * HDIM ** (-0.5)
    logits = jnp.where(allowed, scores, masked_value)
    sink_logit = sink_logits.reshape(kv_local, group_size)[:, :, None, None]
    top_value = jnp.maximum(jnp.max(logits, axis=-1, keepdims=True), sink_logit)
    exponent = jnp.exp(logits - top_value)
    denominator = jnp.sum(exponent, axis=-1, keepdims=True) + jnp.exp(sink_logit - top_value)
    probs = (exponent / denominator).astype(jnp.bfloat16)
    attended = jnp.einsum("kgqj,jkd->qkgd", probs, all_values, preferred_element_type=jnp.float32)
    attended = attended.astype(jnp.bfloat16).reshape(tok_rows, -1)
    projected = lax.psum_scatter(
        jnp.dot(attended, out_weight, preferred_element_type=jnp.float32).astype(jnp.bfloat16),
        "tp",
        scatter_dimension=0,
        tiled=True,
    ).astype(jnp.float32)
    return rms_scale(projected, mix_gain).astype(jnp.bfloat16)


def slot_places(route_rows, experts):
    blocks, tok_rows, top_count = route_rows.shape
    flat_routes = route_rows.reshape(blocks, tok_rows * top_count)
    onehot = (
        flat_routes[:, :, None] == jnp.arange(experts, dtype=jnp.int32)[None, None, :]
    ).astype(jnp.int32)
    earlier = jnp.cumsum(onehot, axis=1) - onehot
    slot_rank = jnp.sum(earlier * onehot, axis=2)
    return (slot_rank * experts + flat_routes).reshape(blocks, tok_rows, top_count)


def dispatch_matrix(slot_place, slots):
    targets = jnp.arange(slots, dtype=jnp.int32)
    hits = (slot_place[:, None, :, :] == targets[None, :, None, None]).astype(jnp.float32)
    return jnp.sum(hits, axis=3).astype(jnp.bfloat16)


def routed_experts(
    moe_tokens, moe_gain, routes, route_weights, expert_gate, expert_up, expert_down
):
    tok_rows, width = moe_tokens.shape
    top_count = routes.shape[1]
    experts = lax.axis_size("ep")
    capacity = tok_rows * top_count * 5 // (4 * experts)
    normed = rms_scale(moe_tokens.astype(jnp.float32), moe_gain).astype(jnp.bfloat16)
    gate_weight = expert_gate[0]
    up_weight = expert_up[0]
    down_weight = expert_down[0]
    slot_place = slot_places(routes[None], experts)
    select_rows = dispatch_matrix(slot_place, capacity * experts)[0]
    outgoing = jnp.dot(select_rows, normed, preferred_element_type=jnp.float32)
    outgoing = outgoing.astype(jnp.bfloat16).reshape(capacity, experts, width)
    slot_rows = lax.all_gather(
        lax.all_to_all(outgoing, "ep", split_axis=1, concat_axis=1, tiled=True),
        "tp",
        axis=0,
        tiled=True,
    )
    gate_value = jnp.dot(slot_rows, gate_weight, preferred_element_type=jnp.float32)
    up_value = jnp.dot(slot_rows, up_weight, preferred_element_type=jnp.float32)
    hidden = (jax.nn.silu(gate_value) * up_value).astype(jnp.bfloat16)
    summed = lax.psum_scatter(
        jnp.dot(hidden, down_weight, preferred_element_type=jnp.float32).astype(jnp.bfloat16),
        "tp",
        scatter_dimension=0,
        tiled=True,
    )
    returned = lax.all_to_all(summed, "ep", split_axis=1, concat_axis=1, tiled=True)
    flat_returned = returned.reshape(capacity * experts, width)
    picked = flat_returned[slot_place[0]]
    combined = jnp.sum(route_weights[:, :, None] * picked.astype(jnp.float32), axis=1)
    return combined.astype(jnp.bfloat16)


def shards(
    queries,
    key_rows,
    value_rows,
    sink_logits,
    out_weight,
    mix_gain,
    moe_tokens,
    moe_gain,
    routes,
    route_weights,
    expert_gate,
    expert_up,
    expert_down,
):
    mixed = mixer(queries, key_rows, value_rows, sink_logits, out_weight, mix_gain)
    moe_out = routed_experts(
        moe_tokens, moe_gain, routes, route_weights, expert_gate, expert_up, expert_down
    )
    return (mixed, moe_out)


def solution(mesh):
    return jax.shard_map(
        shards,
        mesh=mesh,
        in_specs=(
            P("ep", "tp"),
            P("ep", "tp"),
            P("ep", "tp"),
            P("tp"),
            P("tp", None),
            P(),
            P(("ep", "tp"), None),
            P(),
            P(("ep", "tp"), None),
            P(("ep", "tp"), None),
            P("ep", None, "tp"),
            P("ep", None, "tp"),
            P("ep", "tp", None),
        ),
        out_specs=(P(("ep", "tp"), None), P(("ep", "tp"), None)),
        check_vma=False,
    )
```

profile of v0, /device:TPU:0, one launch (start us, length us, event | category | flops | bytes accessed | tf_op | source)
XLA Modules:
  0.0 227.5 jit_solution(6679655546497340957)
XLA Ops:
  7.2 0.8 copy.32
  8.2 0.6 reduce-window.6
  8.8 0.2 slice_reduce_fusion
  9.2 0.1 mul.99
  9.5 1.2 fusion.10
  10.7 1.6 fusion.7
  12.3 0.7 copy.35
  13.1 38.5 %all_to_all.10 = bf16[40,8,2048]{2,0,1:T(8,128)(2,1)S(1)} all-to-all(bf16[40,8,2048]{2,0,1:T(8,128)(2,1)S(1)} %copy.35), channel_id=1, replica_groups=mesh['ep'=8,'tp'=4] {'ep'}, dimensions={1} | all-to-all | bytes 2621440 | tf_op jit(solution)/shard_map/all_to_all | solution.py:96
  51.6 1.8 copy.36
  53.4 39.5 %all-gather.2.cloned.1.call-done = bf16[160,8,2048]{2,1,0:T(8,128)(2,1)} async-done(((bf16[40,8,2048]{2,1,0:T(8,128)(2,1)}), bf16[160,8,2048]{2,1,0:T(8,128)(2,1)}) %all-gather.2.cloned.1.call-update) | async-done | bytes 5242896 | tf_op jit(solution)/shard_map/all_gather | solution.py:95
  92.9 10.0 %fusion.1 = f32[160,8,896]{2,1,0:T(8,128)} fusion(bf16[160,8,2048]{2,1,0:T(8,128)(2,1)} %all-gather.2.cloned.1.call-done, bf16[1,2048,896]{2,1,0:T(8,128)(2,1)} %param.24), kind=kOutput, calls=%fused_computation.4 | convolution fusion | flops 4697620480 | bytes 13500416 | tf_op jit(solution)/shard_map/dot_general | solution.py:102
  102.9 17.3 %convolution_convert_fusion = bf16[160,8,2048]{2,1,0:T(8,128)(2,1)} fusion(bf16[1,896,2048]{2,1,0:T(8,128)(2,1)} %param.25, f32[160,8,896]{2,1,0:T(8,128)} %fusion.1, bf16[160,8,2048]{2,1,0:T(8,128)(2,1)} %all-gather.2.cloned.1.call-done, bf16[1,2048,896]{2,1,0:T(8,128)(2,1)} %param.23), kind=kOutput, calls=%fused_computation.2 | convolution fusion | flops 9404743680 | bytes 22413312 | tf_op jit(solution)/shard_map/dot_general | solution.py:105
  120.3 0.7 copy-done.2
  121.0 3.4 %collective-permute-start.1 = (bf16[128,64]{0,1:T(8,128)(2,1)S(1)}, bf16[128,64]{0,1:T(8,128)(2,1)S(1)}, u32[]{:S(2)}, u32[]{:S(2)}) collective-permute-start(bf16[128,64]{0,1:T(8,128)(2,1)S(1)} %slice.13), channel_id=1, source_target_pairs={{0,4},{4,8},{8,12},{12,16},{16,20},{20,24},{24,28},{1,5},{5,9},{9,... | collective-permute-start | bytes 49160 | tf_op jit(solution)/shard_map/ppermute | solution.py:17
  124.4 3.6 %collective-permute-start = (bf16[128,64]{0,1:T(8,128)(2,1)S(1)}, bf16[128,64]{0,1:T(8,128)(2,1)S(1)}, u32[]{:S(2)}, u32[]{:S(2)}) collective-permute-start(bf16[128,64]{0,1:T(8,128)(2,1)S(1)} %slice.12), channel_id=1, source_target_pairs={{0,4},{4,8},{8,12},{12,16},{16,20},{20,24},{24,28},{1,5},{5,9},{9,... | collective-permute-start | bytes 49160 | tf_op jit(solution)/shard_map/ppermute | solution.py:17
  128.0 0.2 fusion.24
  128.2 0.4 fusion.35
  128.7 0.2 fusion.13
  128.9 0.3 collective-permute-done
  129.2 0.3 convolution_convert_fusion.3
  129.6 1.5 convolution_convert_fusion.2
  131.1 40.7 %reduce-scatter.5.cloned.1.call-done = bf16[40,8,2048]{2,1,0:T(8,128)(2,1)} async-done(((bf16[160,8,2048]{2,1,0:T(8,128)(2,1)}), bf16[40,8,2048]{2,1,0:T(8,128)(2,1)}) %reduce-scatter.5.cloned.1.call-update) | async-done | bytes 1310736 | tf_op jit(solution)/shard_map/reduce_scatter | solution.py:104
  171.8 3.1 %copy.37 = bf16[40,8,2048]{2,0,1:T(8,128)(2,1)} copy(bf16[40,8,2048]{2,1,0:T(8,128)(2,1)} %reduce-scatter.5.cloned.1.call-done) | data formatting | bytes 2621440 | tf_op jit(solution)/shard_map/reduce_scatter | solution.py:104
  174.9 5.5 %all-to-all-start.1 = ((bf16[40,8,2048]{2,0,1:T(8,128)(2,1)}), bf16[40,8,2048]{2,0,1:T(8,128)(2,1)S(1)}, u32[]{:S(2)}, u32[]{:S(2)}) async-start(bf16[40,8,2048]{2,0,1:T(8,128)(2,1)} %copy.37), calls=%async_computation.3 | async-start | bytes 2621440 | tf_op jit(solution)/shard_map/all_to_all | solution.py:110
  180.7 18.5 %reduce-scatter.3.cloned.1.call-done = bf16[64,2048]{1,0:T(8,128)(2,1)} async-done(((bf16[256,2048]{1,0:T(8,128)(2,1)}), bf16[64,2048]{1,0:T(8,128)(2,1)}) %reduce-scatter.3.cloned.1.call-update) | async-done | bytes 262160 | tf_op jit(solution)/shard_map/reduce_scatter | solution.py:54
  199.2 1.1 fusion.17
  200.3 1.8 fusion.19
  202.1 9.6 %all-to-all-done.1 = bf16[40,8,2048]{2,0,1:T(8,128)(2,1)S(1)} async-done(((bf16[40,8,2048]{2,0,1:T(8,128)(2,1)}), bf16[40,8,2048]{2,0,1:T(8,128)(2,1)S(1)}, u32[]{:S(2)}, u32[]{:S(2)}) %all-to-all-start.1) | async-done | bytes 1310752 | tf_op jit(solution)/shard_map/all_to_all | solution.py:110
  211.6 0.7 copy.41
  212.3 2.3 %gather_fusion = bf16[256,2048]{1,0:T(8,128)(2,1)} fusion(bf16[320,2048]{1,0:T(8,128)(2,1)S(1)} %bitcast.65, s32[1024]{0:T(1024)S(1)} %pad_clamp_fusion), kind=kCustom, calls=%fused_computation | custom fusion | bytes 2098176 | tf_op jit(solution)/shard_map/gather | solution.py:112
  214.7 2.4 %reshape.297 = f32[128,2,2048]{2,1,0:T(2,128)S(1)} reshape(bf16[256,2048]{1,0:T(8,128)(2,1)} %gather_fusion) | data formatting | bytes 3145728 | tf_op jit(solution)/shard_map/convert_element_type | solution.py:113
  217.1 3.9 %multiply_reduce_fusion = bf16[128,2048]{1,0:T(8,128)(2,1)} fusion(f32[128,2,2048]{2,1,0:T(2,128)S(1)} %reshape.297, f32[128,2]{1,0:T(8,128)S(1)} %copy.31), kind=kLoop, calls=%fused_computation.11 | loop fusion | flops 786432 | bytes 2622464 | tf_op jit(solution)/shard_map/reduce_sum | solution.py:113
  (41 shorter events, 1.1 us)
Async XLA Ops:
  7.2 122.4 %copy-start = (bf16[192,2048]{1,0:T(8,128)(2,1)S(1)}, bf16[192,2048]{1,0:T(8,128)(2,1)}, u32[]{:S(2)}) copy-start(bf16[192,2048]{1,0:T(8,128)(2,1)} %param.17) | copy-start | bytes 2359300
  7.2 85.8 %all-gather.2.cloned.1.call-start = ((), (), s32[]{:S(2)}) async-start(), calls=%async_computation.5 | async-start | bytes 6553600 | tf_op jit(solution)/shard_map/all_gather | solution.py:95
  53.4 118.4 %reduce-scatter.5.cloned.1.call-start = ((), (), s32[]{:S(2)}) async-start(), calls=%async_computation.6 | async-start | bytes 6553600 | tf_op jit(solution)/shard_map/reduce_scatter | solution.py:104
  120.2 0.8 copy-start.2
  120.2 4.1 %copy-start.3 = (bf16[256,64]{0,1:T(8,128)(2,1)S(1)}, bf16[256,64]{0,1:T(8,128)(2,1)}, u32[]{:S(2)}) copy-start(bf16[256,64]{0,1:T(8,128)(2,1)} %param.15) | copy-start | bytes 98308
  120.2 8.0 %copy-start.6 = (bf16[256,192]{0,1:T(8,128)(2,1)S(1)}, bf16[256,192]{0,1:T(8,128)(2,1)}, u32[]{:S(2)}) copy-start(bf16[256,192]{0,1:T(8,128)(2,1)} %param.13) | copy-start | bytes 294916
  120.2 8.3 %copy-start.4 = (f32[3]{0:T(128)S(1)}, f32[3]{0:T(128)}, u32[]{:S(2)}) copy-start(f32[3]{0:T(128)} %param.16) | copy-start | bytes 40
  120.3 78.9 %reduce-scatter.3.cloned.1.call-start = ((), (), s32[]{:S(2)}) async-start(), calls=%async_computation.4 | async-start | bytes 1310720 | tf_op jit(solution)/shard_map/reduce_scatter | solution.py:54
  121.0 7.2 %collective-permute-start.1 = (bf16[128,64]{0,1:T(8,128)(2,1)S(1)}, bf16[128,64]{0,1:T(8,128)(2,1)S(1)}, u32[]{:S(2)}, u32[]{:S(2)}) collective-permute-start(bf16[128,64]{0,1:T(8,128)(2,1)S(1)} %slice.13), channel_id=1, source_target_pairs={{0,4},{4,8},{8,12},{12,16},{16,20},{20,24},{24,28},{1,5},{5,9},{9,... | collective-permute-start | bytes 49160 | tf_op jit(solution)/shard_map/ppermute | solution.py:17
  124.4 4.8 %collective-permute-start = (bf16[128,64]{0,1:T(8,128)(2,1)S(1)}, bf16[128,64]{0,1:T(8,128)(2,1)S(1)}, u32[]{:S(2)}, u32[]{:S(2)}) collective-permute-start(bf16[128,64]{0,1:T(8,128)(2,1)S(1)} %slice.12), channel_id=1, source_target_pairs={{0,4},{4,8},{8,12},{12,16},{16,20},{20,24},{24,28},{1,5},{5,9},{9,... | collective-permute-start | bytes 49160 | tf_op jit(solution)/shard_map/ppermute | solution.py:17
  129.5 51.0 %copy-start.5 = (f32[128,2]{0,1:T(2,128)S(1)}, f32[128,2]{0,1:T(2,128)}, u32[]{:S(2)}) copy-start(f32[128,2]{0,1:T(2,128)} %param.22) | copy-start | bytes 3076
  131.0 69.2 %copy-start.1 = (f32[2048]{0:T(1024)S(1)}, f32[2048]{0:T(1024)}, u32[]{:S(2)}) copy-start(f32[2048]{0:T(1024)} %param.18) | copy-start | bytes 24580
  174.9 36.7 %all-to-all-start.1 = ((bf16[40,8,2048]{2,0,1:T(8,128)(2,1)}), bf16[40,8,2048]{2,0,1:T(8,128)(2,1)S(1)}, u32[]{:S(2)}, u32[]{:S(2)}) async-start(bf16[40,8,2048]{2,0,1:T(8,128)(2,1)} %copy.37), calls=%async_computation.3 | async-start | bytes 2621440 | tf_op jit(solution)/shard_map/all_to_all | solution.py:110
Sparse Core Ops, SparseCore 0:
  53.5 39.4 all-gather.1
  120.4 51.3 reduce-scatter.4
  174.3 24.7 reduce-scatter.2
where the time goes:
time: 228 us
  waiting for transfers between devices  109 us (48%)
  blocking collectives  38.5 us (17%)
  matrix products  31.1 us (14%)
  between operations  14 us (6%)
  local copies, waits for them, and re-layouts  13.4 us (6%)
  starting transfers between devices  12.6 us (6%)
  other arithmetic  9.38 us (4%)
    reduce_scatter x1, waiting for transfers between devices, routed_experts(): lax.psum_scatter(jnp.dot(hidden, down_weight, preferred_element_type=jnp....  40.7 us
    all_gather x1, waiting for transfers between devices, routed_experts(): lax.all_gather(lax.all_to_all(outgoing, 'ep', split_axis=1, concat_axis=1...  39.5 us
    all_to_all x1, blocking collectives, routed_experts(): lax.all_to_all(outgoing, 'ep', split_axis=1, concat_axis=1, tiled=True)  38.5 us
    reduce_scatter x1, waiting for transfers between devices, mixer(): lax.psum_scatter(jnp.dot(attended, out_weight, preferred_element_type=jnp...  18.5 us
    dot_general x1, matrix products, routed_experts(): jnp.dot(hidden, down_weight, preferred_element_type=jnp.float32)  17.3 us
    dot_general x1, matrix products, routed_experts(): up_value = jnp.dot(slot_rows, up_weight, preferred_element_type=jnp.float32)  9.97 us
    all_to_all x1, waiting for transfers between devices, routed_experts(): lax.all_to_all(summed, 'ep', split_axis=1, concat_axis=1, tiled=True)  9.55 us
    ppermute x2, starting transfers between devices, shifted(): return lax.ppermute(shard, axis, pairs)  6.93 us
  transfers between devices with their start and end apart: 6, of which 5 were waited for; matrix products, arithmetic and copies ran while one was open for 4% of the time, Pallas kernels for 0%

commit v1 on v0

v1 whole, which is shorter than its diff:
```python
import jax
import jax.numpy as jnp
from jax import lax
from jax.sharding import PartitionSpec as P

HDIM = 64
WINDOW = 128

PERMUTE_EP = 8

norm_eps = 1e-06
masked_value = -1e30


def shifted(shard, axis, by):
    size = lax.axis_size(axis)
    pairs = [(i, i + by) for i in range(size) if 0 <= i + by < size]
    return lax.ppermute(shard, axis, pairs)


def crossed(shard, axis, bits):
    size = lax.axis_size(axis)
    return lax.ppermute(shard, axis, [(i, i ^ bits) for i in range(size)])


def rms_scale(rows_in, gain):
    squares = jnp.mean(rows_in * rows_in, axis=-1, keepdims=True)
    return rows_in * lax.rsqrt(squares + norm_eps) * gain


def tp_bits():
    size = lax.axis_size("tp")
    bits = []
    while size > 1:
        size //= 2
        bits.append(size)
    return bits


def tp_gather(rows):
    for bit in tp_bits():
        rows = jnp.concatenate([rows, crossed(rows, "tp", bit)], axis=0)
    return rows


def tp_reduce(partial):
    for bit in reversed(tp_bits()):
        half = partial.shape[0] // 2
        other = crossed(partial[half:], "tp", bit)
        total = partial[:half].astype(jnp.float32) + other.astype(jnp.float32)
        partial = total.astype(jnp.bfloat16)
    return partial


def mixer_local(queries, key_rows, value_rows, sink_logits, out_weight):
    tok_rows = queries.shape[0]
    kv_local = key_rows.shape[1] // HDIM
    group_size = queries.shape[1] // key_rows.shape[1]
    both = jnp.concatenate([key_rows, value_rows], axis=1)
    prev = shifted(both[tok_rows - WINDOW :], "ep", 1)
    kv_cols = key_rows.shape[1]
    all_keys = jnp.concatenate([prev[:, :kv_cols], key_rows], axis=0).reshape(
        tok_rows + WINDOW, kv_local, HDIM
    )
    all_values = jnp.concatenate([prev[:, kv_cols:], value_rows], axis=0).reshape(
        tok_rows + WINDOW, kv_local, HDIM
    )
    offset = lax.axis_index("ep") * tok_rows
    query_pos = offset + jnp.arange(tok_rows, dtype=jnp.int32)
    key_pos = offset - WINDOW + jnp.arange(tok_rows + WINDOW, dtype=jnp.int32)
    distance = query_pos[:, None] - key_pos[None, :]
    allowed = (distance >= 0) & (distance < WINDOW) & (key_pos >= 0)[None, :]
    grouped = queries.reshape(tok_rows, kv_local, group_size, HDIM)
    scores = jnp.einsum(
        "qkgd,jkd->kgqj", grouped, all_keys, preferred_element_type=jnp.float32
    ) * HDIM ** (-0.5)
    logits = jnp.where(allowed, scores, masked_value)
    sink_logit = sink_logits.reshape(kv_local, group_size)[:, :, None, None]
    top_value = jnp.maximum(jnp.max(logits, axis=-1, keepdims=True), sink_logit)
    exponent = jnp.exp(logits - top_value)
    denominator = jnp.sum(exponent, axis=-1, keepdims=True) + jnp.exp(sink_logit - top_value)
    probs = (exponent / denominator).astype(jnp.bfloat16)
    attended = jnp.einsum("kgqj,jkd->qkgd", probs, all_values, preferred_element_type=jnp.float32)
    attended = attended.astype(jnp.bfloat16).reshape(tok_rows, -1)
    return jnp.dot(attended, out_weight, preferred_element_type=jnp.float32).astype(jnp.bfloat16)


def mixer_reduce(partial, mix_gain):
    size = lax.axis_size("tp")
    own = lax.axis_index("tp")
    rows = partial.shape[0] // size
    order = [0]
    for bit in tp_bits():
        order = order + [i ^ bit for i in order]
    blocks = [
        lax.dynamic_slice_in_dim(partial, (own ^ distance) * rows, rows, 0) for distance in order
    ]
    projected = tp_reduce_wide(jnp.concatenate(blocks, axis=0))
    return rms_scale(projected, mix_gain).astype(jnp.bfloat16)


def tp_reduce_wide(partial):
    bits = list(reversed(tp_bits()))
    for number, bit in enumerate(bits):
        half = partial.shape[0] // 2
        other = crossed(partial[half:], "tp", bit)
        total = partial[:half].astype(jnp.float32) + other.astype(jnp.float32)
        if number + 1 < len(bits):
            total = total.astype(jnp.bfloat16)
        partial = total
    return partial


def expert(rows, gate_weight, up_weight, down_weight):
    gate_value = jnp.dot(rows, gate_weight, preferred_element_type=jnp.float32)
    up_value = jnp.dot(rows, up_weight, preferred_element_type=jnp.float32)
    hidden = (jax.nn.silu(gate_value) * up_value).astype(jnp.bfloat16)
    return jnp.dot(hidden, down_weight, preferred_element_type=jnp.float32).astype(jnp.bfloat16)


def route_tables(routes, route_weights, experts, capacity, own):
    tok_rows = routes.shape[0]
    named = jnp.arange(experts, dtype=jnp.int32)[:, None, None] ^ own
    chosen = routes.T[None, :, :] == named
    member = jnp.any(chosen, axis=1)
    weight = jnp.sum(jnp.where(chosen, route_weights.T[None, :, :], 0.0), axis=1)
    token = jnp.arange(tok_rows, dtype=jnp.int32)
    before = (token[:, None] < token[None, :]).astype(jnp.bfloat16)
    earlier = jnp.dot(member.astype(jnp.bfloat16), before, preferred_element_type=jnp.float32)
    rank = jnp.where(member, earlier, -1.0).astype(jnp.int32)
    hits = rank[:, None, :] == jnp.arange(capacity, dtype=jnp.int32)[None, :, None]
    select = hits.astype(jnp.bfloat16)
    spread = jnp.where(hits, weight[:, None, :], 0.0)
    high = spread.astype(jnp.bfloat16)
    low = (spread - high.astype(jnp.float32)).astype(jnp.bfloat16)
    return select, high, low


def shards(
    queries,
    key_rows,
    value_rows,
    sink_logits,
    out_weight,
    mix_gain,
    moe_tokens,
    moe_gain,
    routes,
    route_weights,
    expert_gate,
    expert_up,
    expert_down,
):
    tok_rows, width = moe_tokens.shape
    top_count = routes.shape[1]
    experts = lax.axis_size("ep")
    capacity = tok_rows * top_count * 5 // (4 * experts)
    permuted = experts <= PERMUTE_EP
    own = lax.axis_index("ep") if permuted else jnp.int32(0)
    weights = (expert_gate[0], expert_up[0], expert_down[0])

    select, high, low = route_tables(routes, route_weights, experts, capacity, own)
    normed = rms_scale(moe_tokens.astype(jnp.float32), moe_gain).astype(jnp.bfloat16)
    outgoing = jnp.dot(
        select.reshape(experts * capacity, tok_rows), normed, preferred_element_type=jnp.float32
    )
    outgoing = outgoing.astype(jnp.bfloat16).reshape(experts, capacity, width)

    def combine(first, count, rows):
        cut = slice(first, first + count)
        flat = rows.reshape(count * capacity, width)
        total = None
        for part in (high, low):
            term = lax.dot_general(
                part[cut].reshape(count * capacity, tok_rows),
                flat,
                (((0,), (0,)), ((), ())),
                preferred_element_type=jnp.float32,
            )
            total = term if total is None else total + term
        return total

    partial = mixer_local(queries, key_rows, value_rows, sink_logits, out_weight)
    mixed = mixer_reduce(partial, mix_gain)

    if permuted:
        arrived = []
        for k in range(experts // 2):
            side = crossed(outgoing[2 * k + 1], "ep", 1)
            block = jnp.concatenate([outgoing[2 * k], side], axis=0)
            if k:
                block = crossed(block, "ep", 2 * k)
            arrived.append(block)
        combined = None
        for k, block in enumerate(arrived):
            result = tp_reduce(expert(tp_gather(block), *weights))
            if k:
                result = crossed(result, "ep", 2 * k)
            side = crossed(result[capacity:], "ep", 1)
            term = combine(2 * k, 2, jnp.concatenate([result[:capacity], side], axis=0))
            combined = term if combined is None else combined + term
    else:
        block = lax.all_to_all(outgoing, "ep", split_axis=0, concat_axis=0, tiled=True)
        result = tp_reduce(
            expert(tp_gather(block.reshape(experts * capacity, width)), *weights)
        )
        returned = lax.all_to_all(
            result.reshape(experts, capacity, width), "ep", split_axis=0, concat_axis=0, tiled=True
        )
        combined = combine(0, experts, returned)
    return (mixed, combined.astype(jnp.bfloat16))


def solution(mesh):
    return jax.shard_map(
        shards,
        mesh=mesh,
        in_specs=(
            P("ep", "tp"),
            P("ep", "tp"),
            P("ep", "tp"),
            P("tp"),
            P("tp", None),
            P(),
            P(("ep", "tp"), None),
            P(),
            P(("ep", "tp"), None),
            P(("ep", "tp"), None),
            P("ep", None, "tp"),
            P("ep", None, "tp"),
            P("ep", "tp", None),
        ),
        out_specs=(P(("ep", "tp"), None), P(("ep", "tp"), None)),
        check_vma=False,
    )
```

time: 228 us -> 195 us (0.86)
  waiting for transfers between devices: 109 us -> 68.8 us
  blocking collectives: 38.5 us -> 0 us
  starting transfers between devices: 12.6 us -> 41.7 us
  matrix products: 31.1 us -> 51.9 us
  between operations: 14 us -> 1.28 us
  other arithmetic: 9.38 us -> 13.1 us
  local copies, waits for them, and re-layouts: 13.4 us -> 17 us
    ppermute x0 -> x32, waiting for transfers between devices: none -> 68.8 us  [crossed(): return lax.ppermute(shard, axis, [(i, i ^ bits) for i in range(size)])]
    reduce_scatter x2 -> x0, waiting for transfers between devices: 59.2 us -> none  [the longest x1 40.7 us: routed_experts(): lax.psum_scatter(jnp.dot(hidden, down_weight, preferred_element_type=jnp....]
    all_gather x1 -> x0, waiting for transfers between devices: 39.5 us -> none  [routed_experts(): lax.all_gather(lax.all_to_all(outgoing, 'ep', split_axis=1, concat_axis=1...]
    all_to_all x1 -> x0, blocking collectives: 38.5 us -> none  [routed_experts(): lax.all_to_all(outgoing, 'ep', split_axis=1, concat_axis=1, tiled=True)]
    ppermute x0 -> x32, starting transfers between devices: none -> 36.8 us  [crossed(): return lax.ppermute(shard, axis, [(i, i ^ bits) for i in range(size)])]
    dot_general x6 -> x21, matrix products: 31.1 us -> 51.9 us  [the longest x4 30 us: expert(): jnp.dot(hidden, down_weight, preferred_element_type=jnp.float32)]
    all_to_all x1 -> x0, waiting for transfers between devices: 9.55 us -> none  [routed_experts(): lax.all_to_all(summed, 'ep', split_axis=1, concat_axis=1, tiled=True)]
    slice x3 -> x17, local copies, waits for them, and re-layouts: 0.22 us -> 7.89 us  [the longest x8 6.34 us: tp_reduce(): other = crossed(partial[half:], 'tp', bit)]
  transfers between devices with their start and end apart: 6 -> 33, of which waited for: 5 -> 15; matrix products, arithmetic and copies ran while one was open for 4% -> 39% of each run, Pallas kernels for 0% -> 0%
where the time goes in v1:
time: 195 us; the launch traced here: 194 us
  waiting for transfers between devices  68.8 us (35%)
  matrix products  51.9 us (27%)
  starting transfers between devices  41.7 us (21%)
  local copies, waits for them, and re-layouts  17 us (9%)
  other arithmetic  13.1 us (7%)
    ppermute x32, waiting for transfers between devices, crossed(): return lax.ppermute(shard, axis, [(i, i ^ bits) for i in range(size)])  68.8 us
    ppermute x32, starting transfers between devices, crossed(): return lax.ppermute(shard, axis, [(i, i ^ bits) for i in range(size)])  36.8 us
    dot_general x4, matrix products, expert(): jnp.dot(hidden, down_weight, preferred_element_type=jnp.float32)  30 us
    dot_general x4, matrix products, expert(): up_value = jnp.dot(rows, up_weight, preferred_element_type=jnp.float32)  15.7 us
    slice x8, local copies, waits for them, and re-layouts, tp_reduce(): other = crossed(partial[half:], 'tp', bit)  6.34 us
    unnamed x48, local copies, waits for them, and re-layouts  5.73 us
    ppermute x1, starting transfers between devices, shifted(): return lax.ppermute(shard, axis, pairs)  4.89 us
    convert_element_type x8, other arithmetic, tp_reduce(): partial = total.astype(jnp.bfloat16)  4.37 us
  transfers between devices with their start and end apart: 33, of which 15 were waited for; matrix products, arithmetic and copies ran while one was open for 39% of the time, Pallas kernels for 0%

profile of v1, /device:TPU:0, one launch (start us, length us, event | category | flops | bytes accessed | tf_op | source)
XLA Modules:
  0.0 193.9 jit_solution(4929948826709304069)
XLA Ops:
  1.5 4.9 %collective-permute-start = (bf16[128,128]{0,1:T(8,128)(2,1)S(1)}, bf16[128,128]{0,1:T(8,128)(2,1)S(1)}, u32[]{:S(2)}, u32[]{:S(2)}) collective-permute-start(bf16[128,128]{0,1:T(8,128)(2,1)S(1)} %pad_maximum_fusion.25), channel_id=1, source_target_pairs={{0,4},{4,8},{8,12},{12,16},{16,20},{20,24},{24,28},{1,5},{5,9},{9,... | collective-permute-start | bytes 98312 | tf_op jit(solution)/shard_map/ppermute | solution.py:18
  8.7 1.6 convolution_convert_fusion
  18.3 3.7 %collective-permute-start.26 = (bf16[80,2048]{1,0:T(8,128)(2,1)S(1)}, bf16[80,2048]{1,0:T(8,128)(2,1)S(1)}, u32[]{:S(2)}, u32[]{:S(2)}) collective-permute-start(bf16[80,2048]{1,0:T(8,128)(2,1)S(1)} %pad_maximum_fusion.12), channel_id=1, source_target_pairs={{0,24},{4,28},{8,16},{12,20},{16,8},{20,12},{24,0},{28,4},{1,25},{... | collective-permute-start | bytes 983048 | tf_op jit(solution)/shard_map/ppermute | solution.py:23
  22.0 5.4 %collective-permute-done.3 = bf16[40,2048]{1,0:T(8,128)(2,1)S(1)} collective-permute-done((bf16[40,2048]{1,0:T(8,128)(2,1)S(1)}, bf16[40,2048]{1,0:T(8,128)(2,1)S(1)}, u32[]{:S(2)}, u32[]{:S(2)}) %collective-permute-start.3) | collective-permute-done | bytes 163872 | tf_op jit(solution)/shard_map/ppermute | solution.py:23
  29.9 2.7 %collective-permute-start.18 = (bf16[80,2048]{1,0:T(8,128)(2,1)S(1)}, bf16[80,2048]{1,0:T(8,128)(2,1)S(1)}, u32[]{:S(2)}, u32[]{:S(2)}) collective-permute-start(bf16[80,2048]{1,0:T(8,128)(2,1)S(1)} %pad_maximum_fusion.10), channel_id=1, source_target_pairs={{0,16},{4,20},{8,24},{12,28},{16,0},{20,4},{24,8},{28,12},{1,17},{... | collective-permute-start | bytes 983048 | tf_op jit(solution)/shard_map/ppermute | solution.py:23
  33.5 1.6 collective-permute-start.10
  38.2 12.2 %collective-permute-done.18 = bf16[80,2048]{1,0:T(8,128)(2,1)S(1)} collective-permute-done((bf16[80,2048]{1,0:T(8,128)(2,1)S(1)}, bf16[80,2048]{1,0:T(8,128)(2,1)S(1)}, u32[]{:S(2)}, u32[]{:S(2)}) %collective-permute-start.18) | collective-permute-done | bytes 327712 | tf_op jit(solution)/shard_map/ppermute | solution.py:23
  55.1 5.9 %collective-permute-done.19 = bf16[80,2048]{1,0:T(8,128)(2,1)S(1)} collective-permute-done((bf16[80,2048]{1,0:T(8,128)(2,1)S(1)}, bf16[80,2048]{1,0:T(8,128)(2,1)S(1)}, u32[]{:S(2)}, u32[]{:S(2)}) %collective-permute-start.19) | collective-permute-done | bytes 327712 | tf_op jit(solution)/shard_map/ppermute | solution.py:23
  61.9 6.1 %collective-permute-done.11 = bf16[80,2048]{1,0:T(8,128)(2,1)S(1)} collective-permute-done((bf16[80,2048]{1,0:T(8,128)(2,1)S(1)}, bf16[80,2048]{1,0:T(8,128)(2,1)S(1)}, u32[]{:S(2)}, u32[]{:S(2)}) %collective-permute-start.11) | collective-permute-done | bytes 327712 | tf_op jit(solution)/shard_map/ppermute | solution.py:23
  68.1 4.0 %collective-permute-done.2 = bf16[64,2048]{1,0:T(8,128)(2,1)S(1)} collective-permute-done((bf16[64,2048]{1,0:T(8,128)(2,1)S(1)}, bf16[64,2048]{1,0:T(8,128)(2,1)S(1)}, u32[]{:S(2)}, u32[]{:S(2)}) %collective-permute-start.2) | collective-permute-done | bytes 262176 | tf_op jit(solution)/shard_map/ppermute | solution.py:23
  75.6 2.5 %fusion.14 = f32[320,896]{1,0:T(8,128)} fusion(bf16[1,2048,896]{2,1,0:T(8,128)(2,1)S(1)} %copy-done.18, bf16[160,2048]{1,0:T(8,128)(2,1)S(1)} %collective-permute-done.5, bf16[80,2048]{1,0:T(8,128)(2,1)S(1)} %collective-permute-done.4, bf16[40,2048]{1,0:T(8,128)(2,1)S(1)} %collective-permute-done.3, bf16[40,2048]{1,0:T(8,128)(2,1)S(1)} %get-tuple-element.2), kind=kOutput, calls=%fused_computation.14 | convolution fusion | flops 1179648000 | bytes 6127616 | tf_op jit(solution)/shard_map/dot_general | solution.py:116
  78.1 6.6 %fusion.24 = bf16[320,2048]{1,0:T(8,128)(2,1)S(1)} fusion(bf16[1,896,2048]{2,1,0:T(8,128)(2,1)} %param.25, f32[320,896]{1,0:T(8,128)} %fusion.14, bf16[1,2048,896]{2,1,0:T(8,128)(2,1)} %param.23, bf16[160,2048]{1,0:T(8,128)(2,1)} %copy-done.19, bf16[80,2048]{1,0:T(8,128)(2,1)S(1)} %collective-permute-done.4, ...), kind=kOutput, calls=%fused_computation.25 | convolution fusion | flops 2356428800 | bytes 11108352 | tf_op jit(solution)/shard_map/dot_general | solution.py:118
  85.6 2.0 %constant_dynamic-update-slice_fusion.6 = bf16[320,2048]{1,0:T(8,128)(2,1)} fusion(bf16[320,2048]{1,0:T(8,128)(2,1)} %constant_dynamic-update-slice_fusion.7, bf16[160,2048]{1,0:T(8,128)(2,1)} %collective-permute-done.28), kind=kLoop, calls=%fused_computation.116 | loop fusion | bytes 1310720 | tf_op jit(solution)/shard_map/concatenate | solution.py:42
  87.6 5.0 %fusion.8 = f32[320,896]{1,0:T(8,128)} fusion(bf16[320,2048]{1,0:T(8,128)(2,1)} %constant_dynamic-update-slice_fusion.6, bf16[1,2048,896]{2,1,0:T(8,128)(2,1)} %param.24), kind=kOutput, calls=%fused_computation.8 | convolution fusion | flops 1174405120 | bytes 6127616 | tf_op jit(solution)/shard_map/dot_general | solution.py:116
  92.6 7.8 %fusion.33 = bf16[320,2048]{1,0:T(8,128)(2,1)} fusion(bf16[1,896,2048]{2,1,0:T(8,128)(2,1)} %param.25, f32[320,896]{1,0:T(8,128)} %fusion.8, bf16[320,2048]{1,0:T(8,128)(2,1)} %constant_dynamic-update-slice_fusion.6, bf16[1,2048,896]{2,1,0:T(8,128)(2,1)} %param.23), kind=kOutput, calls=%fused_computation.28 | convolution fusion | flops 2351185920 | bytes 11108352 | tf_op jit(solution)/shard_map/dot_general | solution.py:118
  100.4 2.1 %slice.230 = bf16[160,2048]{1,0:T(8,128)(2,1)} slice(bf16[320,2048]{1,0:T(8,128)(2,1)} %fusion.33), slice={[160:320], [0:2048]} | slice | bytes 1310720 | tf_op jit(solution)/shard_map/slice | solution.py:49
  105.3 4.6 %fusion.10 = f32[320,896]{1,0:T(8,128)} fusion(bf16[320,2048]{1,0:T(8,128)(2,1)S(1)} %constant_dynamic-update-slice_fusion.3, bf16[1,2048,896]{2,1,0:T(8,128)(2,1)} %param.24), kind=kOutput, calls=%fused_computation.10 | convolution fusion | flops 1174405120 | bytes 6127616 | tf_op jit(solution)/shard_map/dot_general | solution.py:116
  109.9 8.0 %fusion.30 = bf16[320,2048]{1,0:T(8,128)(2,1)} fusion(bf16[1,896,2048]{2,1,0:T(8,128)(2,1)} %param.25, f32[320,896]{1,0:T(8,128)} %fusion.10, bf16[320,2048]{1,0:T(8,128)(2,1)} %copy-done.10, bf16[1,2048,896]{2,1,0:T(8,128)(2,1)} %param.23), kind=kOutput, calls=%fused_computation.27 | convolution fusion | flops 2351185920 | bytes 11108352 | tf_op jit(solution)/shard_map/dot_general | solution.py:118
  117.9 2.1 %slice.220 = bf16[160,2048]{1,0:T(8,128)(2,1)} slice(bf16[320,2048]{1,0:T(8,128)(2,1)} %fusion.30), slice={[160:320], [0:2048]} | slice | bytes 1310720 | tf_op jit(solution)/shard_map/slice | solution.py:49
  121.2 3.6 %fusion.12 = f32[320,896]{1,0:T(8,128)S(1)} fusion(bf16[320,2048]{1,0:T(8,128)(2,1)S(1)} %constant_dynamic-update-slice_fusion, bf16[1,2048,896]{2,1,0:T(8,128)(2,1)} %param.24), kind=kOutput, calls=%fused_computation.12 | convolution fusion | flops 1174405120 | bytes 6127616 | tf_op jit(solution)/shard_map/dot_general | solution.py:116
  124.8 7.6 %fusion.27 = bf16[320,2048]{1,0:T(8,128)(2,1)} fusion(bf16[1,896,2048]{2,1,0:T(8,128)(2,1)} %param.25, f32[320,896]{1,0:T(8,128)S(1)} %fusion.12, bf16[320,2048]{1,0:T(8,128)(2,1)} %copy-done.7, bf16[1,2048,896]{2,1,0:T(8,128)(2,1)} %param.23), kind=kOutput, calls=%fused_computation.26 | convolution fusion | flops 2351185920 | bytes 11108352 | tf_op jit(solution)/shard_map/dot_general | solution.py:118
  141.8 4.3 %collective-permute-done.7 = bf16[80,2048]{1,0:T(8,128)(2,1)S(1)} collective-permute-done((bf16[80,2048]{1,0:T(8,128)(2,1)S(1)}, bf16[80,2048]{1,0:T(8,128)(2,1)S(1)}, u32[]{:S(2)}, u32[]{:S(2)}) %collective-permute-start.7) | collective-permute-done | bytes 327712 | tf_op jit(solution)/shard_map/ppermute | solution.py:23
  146.2 1.6 collective-permute-start.8
  149.5 2.0 %collective-permute-done.8 = bf16[40,2048]{1,0:T(8,128)(2,1)S(1)} collective-permute-done((bf16[40,2048]{1,0:T(8,128)(2,1)S(1)}, bf16[40,2048]{1,0:T(8,128)(2,1)S(1)}, u32[]{:S(2)}, u32[]{:S(2)}) %collective-permute-start.8) | collective-permute-done | bytes 163872 | tf_op jit(solution)/shard_map/ppermute | solution.py:23
  153.2 2.5 %collective-permute-start.31 = (bf16[80,2048]{1,0:T(8,128)(2,1)S(1)}, bf16[80,2048]{1,0:T(8,128)(2,1)S(1)}, u32[]{:S(2)}, u32[]{:S(2)}) collective-permute-start(bf16[80,2048]{1,0:T(8,128)(2,1)S(1)} %add_convert_fusion.5), channel_id=1, source_target_pairs={{0,24},{4,28},{8,16},{12,20},{16,8},{20,12},{24,0},{28,4},{1,25},{... | collective-permute-start | bytes 983048 | tf_op jit(solution)/shard_map/ppermute | solution.py:23
  155.7 4.4 %collective-permute-done.22 = bf16[80,2048]{1,0:T(8,128)(2,1)S(1)} collective-permute-done((bf16[80,2048]{1,0:T(8,128)(2,1)S(1)}, bf16[80,2048]{1,0:T(8,128)(2,1)S(1)}, u32[]{:S(2)}, u32[]{:S(2)}) %collective-permute-start.22) | collective-permute-done | bytes 327712 | tf_op jit(solution)/shard_map/ppermute | solution.py:23
  160.2 2.4 %collective-permute-start.23 = (bf16[80,2048]{1,0:T(8,128)(2,1)S(1)}, bf16[80,2048]{1,0:T(8,128)(2,1)S(1)}, u32[]{:S(2)}, u32[]{:S(2)}) collective-permute-start(bf16[80,2048]{1,0:T(8,128)(2,1)S(1)} %add_convert_fusion.6), channel_id=1, source_target_pairs={{0,16},{4,20},{8,24},{12,28},{16,0},{20,4},{24,8},{28,12},{1,17},{... | collective-permute-start | bytes 983048 | tf_op jit(solution)/shard_map/ppermute | solution.py:23
  162.6 3.7 %collective-permute-done.14 = bf16[80,2048]{1,0:T(8,128)(2,1)S(1)} collective-permute-done((bf16[80,2048]{1,0:T(8,128)(2,1)S(1)}, bf16[80,2048]{1,0:T(8,128)(2,1)S(1)}, u32[]{:S(2)}, u32[]{:S(2)}) %collective-permute-start.14) | collective-permute-done | bytes 327712 | tf_op jit(solution)/shard_map/ppermute | solution.py:23
  167.7 1.6 collective-permute-start.32
  169.3 13.7 %collective-permute-done.23 = bf16[80,2048]{1,0:T(8,128)(2,1)S(1)} collective-permute-done((bf16[80,2048]{1,0:T(8,128)(2,1)S(1)}, bf16[80,2048]{1,0:T(8,128)(2,1)S(1)}, u32[]{:S(2)}, u32[]{:S(2)}) %collective-permute-start.23) | collective-permute-done | bytes 327712 | tf_op jit(solution)/shard_map/ppermute | solution.py:23
  183.1 1.6 collective-permute-start.24
  185.9 4.0 %collective-permute-done.24 = bf16[40,2048]{1,0:T(8,128)(2,1)S(1)} collective-permute-done((bf16[40,2048]{1,0:T(8,128)(2,1)S(1)}, bf16[40,2048]{1,0:T(8,128)(2,1)S(1)}, u32[]{:S(2)}, u32[]{:S(2)}) %collective-permute-start.24) | collective-permute-done | bytes 163872 | tf_op jit(solution)/shard_map/ppermute | solution.py:23
  (163 shorter events, 50.9 us)
Async XLA Ops:
  1.5 14.8 %collective-permute-start = (bf16[128,128]{0,1:T(8,128)(2,1)S(1)}, bf16[128,128]{0,1:T(8,128)(2,1)S(1)}, u32[]{:S(2)}, u32[]{:S(2)}) collective-permute-start(bf16[128,128]{0,1:T(8,128)(2,1)S(1)} %pad_maximum_fusion.25), channel_id=1, source_target_pairs={{0,4},{4,8},{8,12},{12,16},{16,20},{20,24},{24,28},{1,5},{5,9},{9,... | collective-permute-start | bytes 98312 | tf_op jit(solution)/shard_map/ppermute | solution.py:18
  11.2 7.1 %collective-permute-start.25 = (bf16[40,2048]{1,0:T(8,128)(2,1)S(1)}, bf16[40,2048]{1,0:T(8,128)(2,1)S(1)}, u32[]{:S(2)}, u32[]{:S(2)}) collective-permute-start(bf16[40,2048]{1,0:T(8,128)(2,1)S(1)} %get-tuple-element.3), channel_id=1, source_target_pairs={{0,4},{4,0},{8,12},{12,8},{16,20},{20,16},{24,28},{28,24},{1,5},{5... | collective-permute-start | bytes 491528 | tf_op jit(solution)/shard_map/ppermute | solution.py:23
  12.7 16.3 %collective-permute-start.17 = (bf16[40,2048]{1,0:T(8,128)(2,1)S(1)}, bf16[40,2048]{1,0:T(8,128)(2,1)}, u32[]{:S(2)}, u32[]{:S(2)}) collective-permute-start(bf16[40,2048]{1,0:T(8,128)(2,1)S(1)} %get-tuple-element.5), channel_id=1, source_target_pairs={{0,4},{4,0},{8,12},{12,8},{16,20},{20,16},{24,28},{28,24},{1,5},{5... | collective-permute-start | bytes 491528 | tf_op jit(solution)/shard_map/ppermute | solution.py:23
  13.2 19.4 %collective-permute-start.9 = (bf16[40,2048]{1,0:T(8,128)(2,1)}, bf16[40,2048]{1,0:T(8,128)(2,1)}, u32[]{:S(2)}, u32[]{:S(2)}) collective-permute-start(bf16[40,2048]{1,0:T(8,128)(2,1)} %get-tuple-element.7), channel_id=1, source_target_pairs={{0,4},{4,0},{8,12},{12,8},{16,20},{20,16},{24,28},{28,24},{1,5},{5... | collective-permute-start | bytes 491528 | tf_op jit(solution)/shard_map/ppermute | solution.py:23
  14.8 12.6 %collective-permute-start.3 = (bf16[40,2048]{1,0:T(8,128)(2,1)S(1)}, bf16[40,2048]{1,0:T(8,128)(2,1)S(1)}, u32[]{:S(2)}, u32[]{:S(2)}) collective-permute-start(bf16[40,2048]{1,0:T(8,128)(2,1)S(1)} %get-tuple-element.9), channel_id=1, source_target_pairs={{0,4},{4,0},{8,12},{12,8},{16,20},{20,16},{24,28},{28,24},{1,5},{5... | collective-permute-start | bytes 491528 | tf_op jit(solution)/shard_map/ppermute | solution.py:23
  18.0 34.5 %collective-permute-start.1 = (bf16[128,2048]{1,0:T(8,128)(2,1)S(1)}, bf16[128,2048]{1,0:T(8,128)(2,1)S(1)}, u32[]{:S(2)}, u32[]{:S(2)}) collective-permute-start(bf16[128,2048]{1,0:T(8,128)(2,1)S(1)} %pad_maximum_fusion.5), channel_id=1, source_target_pairs={{0,1},{1,0},{2,3},{3,2},{4,5},{5,4},{6,7},{7,6},{8,9},{9,8},{10,11... | collective-permute-start | bytes 1572872 | tf_op jit(solution)/shard_map/ppermute | solution.py:23
  18.3 17.6 %collective-permute-start.26 = (bf16[80,2048]{1,0:T(8,128)(2,1)S(1)}, bf16[80,2048]{1,0:T(8,128)(2,1)S(1)}, u32[]{:S(2)}, u32[]{:S(2)}) collective-permute-start(bf16[80,2048]{1,0:T(8,128)(2,1)S(1)} %pad_maximum_fusion.12), channel_id=1, source_target_pairs={{0,24},{4,28},{8,16},{12,20},{16,8},{20,12},{24,0},{28,4},{1,25},{... | collective-permute-start | bytes 983048 | tf_op jit(solution)/shard_map/ppermute | solution.py:23
  27.4 8.4 %collective-permute-start.4 = (bf16[80,2048]{1,0:T(8,128)(2,1)S(1)}, bf16[80,2048]{1,0:T(8,128)(2,1)S(1)}, u32[]{:S(2)}, u32[]{:S(2)}) collective-permute-start(bf16[80,2048]{1,0:T(8,128)(2,1)S(1)} %pad_maximum_fusion.6), channel_id=1, source_target_pairs={{0,2},{1,3},{2,0},{3,1},{4,6},{5,7},{6,4},{7,5},{8,10},{9,11},{10,... | collective-permute-start | bytes 983048 | tf_op jit(solution)/shard_map/ppermute | solution.py:23
  29.9 20.5 %collective-permute-start.18 = (bf16[80,2048]{1,0:T(8,128)(2,1)S(1)}, bf16[80,2048]{1,0:T(8,128)(2,1)S(1)}, u32[]{:S(2)}, u32[]{:S(2)}) collective-permute-start(bf16[80,2048]{1,0:T(8,128)(2,1)S(1)} %pad_maximum_fusion.10), channel_id=1, source_target_pairs={{0,16},{4,20},{8,24},{12,28},{16,0},{20,4},{24,8},{28,12},{1,17},{... | collective-permute-start | bytes 983048 | tf_op jit(solution)/shard_map/ppermute | solution.py:23
  33.5 18.4 %collective-permute-start.10 = (bf16[80,2048]{1,0:T(8,128)(2,1)S(1)}, bf16[80,2048]{1,0:T(8,128)(2,1)S(1)}, u32[]{:S(2)}, u32[]{:S(2)}) collective-permute-start(bf16[80,2048]{1,0:T(8,128)(2,1)S(1)} %pad_maximum_fusion.8), channel_id=1, source_target_pairs={{0,8},{4,12},{8,0},{12,4},{16,24},{20,28},{24,16},{28,20},{1,9},{5... | collective-permute-start | bytes 983048 | tf_op jit(solution)/shard_map/ppermute | solution.py:23
  35.9 38.8 %collective-permute-start.5 = (bf16[160,2048]{1,0:T(8,128)(2,1)S(1)}, bf16[160,2048]{1,0:T(8,128)(2,1)S(1)}, u32[]{:S(2)}, u32[]{:S(2)}) collective-permute-start(bf16[160,2048]{1,0:T(8,128)(2,1)S(1)} %pad_maximum_fusion.1), channel_id=1, source_target_pairs={{0,1},{1,0},{2,3},{3,2},{4,5},{5,4},{6,7},{7,6},{8,9},{9,8},{10,11... | collective-permute-start | bytes 1966088 | tf_op jit(solution)/shard_map/ppermute | solution.py:23
  36.7 17.5 %collective-permute-start.27 = (bf16[80,2048]{1,0:T(8,128)(2,1)S(1)}, bf16[80,2048]{1,0:T(8,128)(2,1)S(1)}, u32[]{:S(2)}, u32[]{:S(2)}) collective-permute-start(bf16[80,2048]{1,0:T(8,128)(2,1)S(1)} %collective-permute-done.26), channel_id=1, source_target_pairs={{0,2},{1,3},{2,0},{3,1},{4,6},{5,7},{6,4},{7,5},{8,10},{9,11},{10,... | collective-permute-start | bytes 983048 | tf_op jit(solution)/shard_map/ppermute | solution.py:23
  50.4 10.6 %collective-permute-start.19 = (bf16[80,2048]{1,0:T(8,128)(2,1)S(1)}, bf16[80,2048]{1,0:T(8,128)(2,1)S(1)}, u32[]{:S(2)}, u32[]{:S(2)}) collective-permute-start(bf16[80,2048]{1,0:T(8,128)(2,1)S(1)} %collective-permute-done.18), channel_id=1, source_target_pairs={{0,2},{1,3},{2,0},{3,1},{4,6},{5,7},{6,4},{7,5},{8,10},{9,11},{10,... | collective-permute-start | bytes 983048 | tf_op jit(solution)/shard_map/ppermute | solution.py:23
  51.9 16.1 %collective-permute-start.11 = (bf16[80,2048]{1,0:T(8,128)(2,1)S(1)}, bf16[80,2048]{1,0:T(8,128)(2,1)S(1)}, u32[]{:S(2)}, u32[]{:S(2)}) collective-permute-start(bf16[80,2048]{1,0:T(8,128)(2,1)S(1)} %collective-permute-done.10), channel_id=1, source_target_pairs={{0,2},{1,3},{2,0},{3,1},{4,6},{5,7},{6,4},{7,5},{8,10},{9,11},{10,... | collective-permute-start | bytes 983048 | tf_op jit(solution)/shard_map/ppermute | solution.py:23
  52.6 19.5 %collective-permute-start.2 = (bf16[64,2048]{1,0:T(8,128)(2,1)S(1)}, bf16[64,2048]{1,0:T(8,128)(2,1)S(1)}, u32[]{:S(2)}, u32[]{:S(2)}) collective-permute-start(bf16[64,2048]{1,0:T(8,128)(2,1)S(1)} %slice.195), channel_id=1, source_target_pairs={{0,2},{1,3},{2,0},{3,1},{4,6},{5,7},{6,4},{7,5},{8,10},{9,11},{10,... | collective-permute-start | bytes 786440 | tf_op jit(solution)/shard_map/ppermute | solution.py:23
  55.1 30.5 %collective-permute-start.28 = (bf16[160,2048]{1,0:T(8,128)(2,1)}, bf16[160,2048]{1,0:T(8,128)(2,1)}, u32[]{:S(2)}, u32[]{:S(2)}) collective-permute-start(bf16[160,2048]{1,0:T(8,128)(2,1)} %pad_maximum_fusion.4), channel_id=1, source_target_pairs={{0,1},{1,0},{2,3},{3,2},{4,5},{5,4},{6,7},{7,6},{8,9},{9,8},{10,11... | collective-permute-start | bytes 1966088 | tf_op jit(solution)/shard_map/ppermute | solution.py:23
  61.9 41.1 %collective-permute-start.20 = (bf16[160,2048]{1,0:T(8,128)(2,1)}, bf16[160,2048]{1,0:T(8,128)(2,1)}, u32[]{:S(2)}, u32[]{:S(2)}) collective-permute-start(bf16[160,2048]{1,0:T(8,128)(2,1)} %pad_maximum_fusion.3), channel_id=1, source_target_pairs={{0,1},{1,0},{2,3},{3,2},{4,5},{5,4},{6,7},{7,6},{8,9},{9,8},{10,11... | collective-permute-start | bytes 1966088 | tf_op jit(solution)/shard_map/ppermute | solution.py:23
  68.1 52.0 %collective-permute-start.12 = (bf16[160,2048]{1,0:T(8,128)(2,1)S(1)}, bf16[160,2048]{1,0:T(8,128)(2,1)S(1)}, u32[]{:S(2)}, u32[]{:S(2)}) collective-permute-start(bf16[160,2048]{1,0:T(8,128)(2,1)S(1)} %pad_maximum_fusion.2), channel_id=1, source_target_pairs={{0,1},{1,0},{2,3},{3,2},{4,5},{5,4},{6,7},{7,6},{8,9},{9,8},{10,11... | collective-permute-start | bytes 1966088 | tf_op jit(solution)/shard_map/ppermute | solution.py:23
  85.6 48.5 %collective-permute-start.6 = (bf16[160,2048]{1,0:T(8,128)(2,1)}, bf16[160,2048]{1,0:T(8,128)(2,1)}, u32[]{:S(2)}, u32[]{:S(2)}) collective-permute-start(bf16[160,2048]{1,0:T(8,128)(2,1)} %slice.200), channel_id=1, source_target_pairs={{0,1},{1,0},{2,3},{3,2},{4,5},{5,4},{6,7},{7,6},{8,9},{9,8},{10,11... | collective-permute-start | bytes 1966088 | tf_op jit(solution)/shard_map/ppermute | solution.py:23
  102.5 34.5 %collective-permute-start.29 = (bf16[160,2048]{1,0:T(8,128)(2,1)}, bf16[160,2048]{1,0:T(8,128)(2,1)}, u32[]{:S(2)}, u32[]{:S(2)}) collective-permute-start(bf16[160,2048]{1,0:T(8,128)(2,1)} %slice.230), channel_id=1, source_target_pairs={{0,1},{1,0},{2,3},{3,2},{4,5},{5,4},{6,7},{7,6},{8,9},{9,8},{10,11... | collective-permute-start | bytes 1966088 | tf_op jit(solution)/shard_map/ppermute | solution.py:23
  120.0 18.9 %collective-permute-start.21 = (bf16[160,2048]{1,0:T(8,128)(2,1)}, bf16[160,2048]{1,0:T(8,128)(2,1)}, u32[]{:S(2)}, u32[]{:S(2)}) collective-permute-start(bf16[160,2048]{1,0:T(8,128)(2,1)} %slice.220), channel_id=1, source_target_pairs={{0,1},{1,0},{2,3},{3,2},{4,5},{5,4},{6,7},{7,6},{8,9},{9,8},{10,11... | collective-permute-start | bytes 1966088 | tf_op jit(solution)/shard_map/ppermute | solution.py:23
  133.5 14.3 %collective-permute-start.13 = (bf16[160,2048]{1,0:T(8,128)(2,1)S(1)}, bf16[160,2048]{1,0:T(8,128)(2,1)S(1)}, u32[]{:S(2)}, u32[]{:S(2)}) collective-permute-start(bf16[160,2048]{1,0:T(8,128)(2,1)S(1)} %slice.210), channel_id=1, source_target_pairs={{0,1},{1,0},{2,3},{3,2},{4,5},{5,4},{6,7},{7,6},{8,9},{9,8},{10,11... | collective-permute-start | bytes 1966088 | tf_op jit(solution)/shard_map/ppermute | solution.py:23
  135.4 10.6 %collective-permute-start.7 = (bf16[80,2048]{1,0:T(8,128)(2,1)S(1)}, bf16[80,2048]{1,0:T(8,128)(2,1)S(1)}, u32[]{:S(2)}, u32[]{:S(2)}) collective-permute-start(bf16[80,2048]{1,0:T(8,128)(2,1)S(1)} %slice.202), channel_id=1, source_target_pairs={{0,2},{1,3},{2,0},{3,1},{4,6},{5,7},{6,4},{7,5},{8,10},{9,11},{10,... | collective-permute-start | bytes 983048 | tf_op jit(solution)/shard_map/ppermute | solution.py:23
  138.3 14.8 %collective-permute-start.30 = (bf16[80,2048]{1,0:T(8,128)(2,1)S(1)}, bf16[80,2048]{1,0:T(8,128)(2,1)S(1)}, u32[]{:S(2)}, u32[]{:S(2)}) collective-permute-start(bf16[80,2048]{1,0:T(8,128)(2,1)S(1)} %slice.232), channel_id=1, source_target_pairs={{0,2},{1,3},{2,0},{3,1},{4,6},{5,7},{6,4},{7,5},{8,10},{9,11},{10,... | collective-permute-start | bytes 983048 | tf_op jit(solution)/shard_map/ppermute | solution.py:23
  140.2 19.9 %collective-permute-start.22 = (bf16[80,2048]{1,0:T(8,128)(2,1)S(1)}, bf16[80,2048]{1,0:T(8,128)(2,1)S(1)}, u32[]{:S(2)}, u32[]{:S(2)}) collective-permute-start(bf16[80,2048]{1,0:T(8,128)(2,1)S(1)} %slice.222), channel_id=1, source_target_pairs={{0,2},{1,3},{2,0},{3,1},{4,6},{5,7},{6,4},{7,5},{8,10},{9,11},{10,... | collective-permute-start | bytes 983048 | tf_op jit(solution)/shard_map/ppermute | solution.py:23
  148.0 18.3 %collective-permute-start.14 = (bf16[80,2048]{1,0:T(8,128)(2,1)S(1)}, bf16[80,2048]{1,0:T(8,128)(2,1)S(1)}, u32[]{:S(2)}, u32[]{:S(2)}) collective-permute-start(bf16[80,2048]{1,0:T(8,128)(2,1)S(1)} %slice.212), channel_id=1, source_target_pairs={{0,2},{1,3},{2,0},{3,1},{4,6},{5,7},{6,4},{7,5},{8,10},{9,11},{10,... | collective-permute-start | bytes 983048 | tf_op jit(solution)/shard_map/ppermute | solution.py:23
  153.2 14.6 %collective-permute-start.31 = (bf16[80,2048]{1,0:T(8,128)(2,1)S(1)}, bf16[80,2048]{1,0:T(8,128)(2,1)S(1)}, u32[]{:S(2)}, u32[]{:S(2)}) collective-permute-start(bf16[80,2048]{1,0:T(8,128)(2,1)S(1)} %add_convert_fusion.5), channel_id=1, source_target_pairs={{0,24},{4,28},{8,16},{12,20},{16,8},{20,12},{24,0},{28,4},{1,25},{... | collective-permute-start | bytes 983048 | tf_op jit(solution)/shard_map/ppermute | solution.py:23
  160.2 22.8 %collective-permute-start.23 = (bf16[80,2048]{1,0:T(8,128)(2,1)S(1)}, bf16[80,2048]{1,0:T(8,128)(2,1)S(1)}, u32[]{:S(2)}, u32[]{:S(2)}) collective-permute-start(bf16[80,2048]{1,0:T(8,128)(2,1)S(1)} %add_convert_fusion.6), channel_id=1, source_target_pairs={{0,16},{4,20},{8,24},{12,28},{16,0},{20,4},{24,8},{28,12},{1,17},{... | collective-permute-start | bytes 983048 | tf_op jit(solution)/shard_map/ppermute | solution.py:23
  166.3 18.3 %collective-permute-start.15 = (bf16[80,2048]{1,0:T(8,128)(2,1)S(1)}, bf16[80,2048]{1,0:T(8,128)(2,1)S(1)}, u32[]{:S(2)}, u32[]{:S(2)}) collective-permute-start(bf16[80,2048]{1,0:T(8,128)(2,1)S(1)} %add_convert_fusion.7), channel_id=1, source_target_pairs={{0,8},{4,12},{8,0},{12,4},{16,24},{20,28},{24,16},{28,20},{1,9},{5... | collective-permute-start | bytes 983048 | tf_op jit(solution)/shard_map/ppermute | solution.py:23
  167.7 17.5 %collective-permute-start.32 = (bf16[40,2048]{1,0:T(8,128)(2,1)S(1)}, bf16[40,2048]{1,0:T(8,128)(2,1)S(1)}, u32[]{:S(2)}, u32[]{:S(2)}) collective-permute-start(bf16[40,2048]{1,0:T(8,128)(2,1)S(1)} %get-tuple-element.21), channel_id=1, source_target_pairs={{0,4},{4,0},{8,12},{12,8},{16,20},{20,16},{24,28},{28,24},{1,5},{5... | collective-permute-start | bytes 491528 | tf_op jit(solution)/shard_map/ppermute | solution.py:23
  183.1 6.9 %collective-permute-start.24 = (bf16[40,2048]{1,0:T(8,128)(2,1)S(1)}, bf16[40,2048]{1,0:T(8,128)(2,1)S(1)}, u32[]{:S(2)}, u32[]{:S(2)}) collective-permute-start(bf16[40,2048]{1,0:T(8,128)(2,1)S(1)} %get-tuple-element.19), channel_id=1, source_target_pairs={{0,4},{4,0},{8,12},{12,8},{16,20},{20,16},{24,28},{28,24},{1,5},{5... | collective-permute-start | bytes 491528 | tf_op jit(solution)/shard_map/ppermute | solution.py:23
  184.7 7.0 %collective-permute-start.16 = (bf16[40,2048]{1,0:T(8,128)(2,1)S(1)}, bf16[40,2048]{1,0:T(8,128)(2,1)S(1)}, u32[]{:S(2)}, u32[]{:S(2)}) collective-permute-start(bf16[40,2048]{1,0:T(8,128)(2,1)S(1)} %get-tuple-element.17), channel_id=1, source_target_pairs={{0,4},{4,0},{8,12},{12,8},{16,20},{20,16},{24,28},{28,24},{1,5},{5... | collective-permute-start | bytes 491528 | tf_op jit(solution)/shard_map/ppermute | solution.py:23
  (22 other events, 90.2 us)
